TPU v7x, 32 devices: a whole 2x2x4 slice. The times are simulated.
32 devices in a mesh: rep: 2 (over x), fs: 4 (over z), tp: 4 (over y, core).
Axes of the slice: x: 2, y: 2, z: 4, core: 2. Of those that a mesh axis runs over, the one named last changes fastest.
Arguments:
- tokens: bfloat16 [4096, 2048], P(('rep', 'fs', 'tp')), may hold values from -6 to 6
- norm1_gain: float32 [2048], replicated, may hold values from 0.1 to 1.9
- in_weight: bfloat16 [2048, 1024], P('fs', 'tp'), may hold values from -0.125 to 0.125
- group_weight: bfloat16 [8, 128, 128], P('tp'), may hold values from -0.5 to 0.5
- pool_scale: float32 [1024], P('tp'), may hold values from 0.1 to 1.9
- out_weight: bfloat16 [1024, 2048], P('tp', 'fs'), may hold values from -0.1875 to 0.1875
- norm2_gain: float32 [2048], replicated, may hold values from 0.1 to 1.9
- up_weight: bfloat16 [2048, 8192], P('fs', 'tp'), may hold values from -0.125 to 0.125
- down_weight: bfloat16 [8192, 2048], P('tp', 'fs'), may hold values from -0.0625 to 0.0625
Outputs:
- layer_out: bfloat16 [4096, 2048], P(('rep', 'fs', 'tp'))
All inputs are finite; a program needn't handle non-finite values.
Results may differ from a plain program's by a relative error of at most 0.02.
Values may be sent and summed in bfloat16 or wider, within the bound.
A program may use at most 128 MiB of HBM per device.

v0:
```python
import jax
import jax.numpy as jnp
from jax import lax
from jax.sharding import PartitionSpec as P

GROUP_DIM = 128
epsilon = 1e-06


def rms_norm(values, gain):
    scale = lax.rsqrt(jnp.mean(values * values, axis=-1, keepdims=True) + epsilon)
    return values * scale * gain


def shifted(values, offset):
    return jnp.pad(values, ((offset, 0), (0, 0)))[: values.shape[0]]


def mix_groups(projected, group_weight, pool_scale):
    length = projected.shape[0]
    local_groups = group_weight.shape[0]
    values = projected.astype(jnp.float32)
    level_sums = []
    running = values
    offset = 1
    for level in range(4):
        running = running + shifted(running, offset)
        offset = offset * 2
        level_sums.append(running)
    first_group = lax.axis_index("tp") * local_groups
    group_level = (first_group + jnp.arange(local_groups, dtype=jnp.int32)) % 4
    column_level = jnp.repeat(group_level, GROUP_DIM)[None, :]
    position = jnp.arange(length, dtype=jnp.int32)[:, None]
    window_mean = jnp.zeros_like(values)
    for level in range(4):
        count = jnp.minimum(position + 1, 2 ** (level + 1)).astype(jnp.float32)
        window_mean = jnp.where(column_level == level, level_sums[level] / count, window_mean)
    pooled = (window_mean - values).astype(jnp.bfloat16).reshape(length, local_groups, GROUP_DIM)
    mapped = jnp.einsum("sgc,gcd->sgd", pooled, group_weight, preferred_element_type=jnp.float32)
    return (mapped.reshape(length, local_groups * GROUP_DIM) * pool_scale).astype(jnp.bfloat16)


def local(
    tokens,
    norm1_gain,
    in_weight,
    group_weight,
    pool_scale,
    out_weight,
    norm2_gain,
    up_weight,
    down_weight,
):
    stream = tokens.astype(jnp.float32)
    normed = rms_norm(stream, norm1_gain).astype(jnp.bfloat16)
    in_local = lax.all_gather(in_weight, "fs", axis=0, tiled=True)
    projected = jnp.dot(
        lax.all_gather(normed, "tp", axis=0, tiled=True),
        in_local,
        preferred_element_type=jnp.float32,
    ).astype(jnp.bfloat16)
    pool_out = mix_groups(projected, group_weight, pool_scale)
    out_local = lax.all_gather(out_weight, "fs", axis=1, tiled=True)
    block_rows = pool_out
    mixed = lax.psum_scatter(
        jnp.dot(block_rows, out_local, preferred_element_type=jnp.float32).astype(jnp.bfloat16),
        "tp",
        scatter_dimension=0,
        tiled=True,
    ).astype(jnp.float32)
    mixed_stream = stream + mixed
    normed_two = rms_norm(mixed_stream, norm2_gain).astype(jnp.bfloat16)
    up_local = lax.all_gather(up_weight, "fs", axis=0, tiled=True)
    upper = jnp.dot(
        lax.all_gather(normed_two, "tp", axis=0, tiled=True),
        up_local,
        preferred_element_type=jnp.float32,
    )
    hidden = jnp.square(jax.nn.relu(upper)).astype(jnp.bfloat16)
    down_local = lax.all_gather(down_weight, "fs", axis=1, tiled=True)
    block_rows = hidden
    channel_sum = lax.psum_scatter(
        jnp.dot(block_rows, down_local, preferred_element_type=jnp.float32).astype(jnp.bfloat16),
        "tp",
        scatter_dimension=0,
        tiled=True,
    ).astype(jnp.float32)
    return (mixed_stream + channel_sum).astype(jnp.bfloat16)


def solution(mesh):
    in_specs = (
        P(("rep", "fs", "tp"), None),
        P(),
        P("fs", "tp"),
        P("tp", None, None),
        P("tp"),
        P("tp", "fs"),
        P(),
        P("fs", "tp"),
        P("tp", "fs"),
    )
    out_specs = P(("rep", "fs", "tp"), None)
    return jax.shard_map(local, mesh=mesh, in_specs=in_specs, out_specs=out_specs, check_vma=False)
```

profile of v0, /device:TPU:0, one launch (start us, length us, event | category | flops | bytes accessed | tf_op | source)
XLA Modules:
  0.0 508.3 jit_solution(7314951836628832567)
XLA Ops:
  6.5 0.0 copy-start
  6.5 0.0 all-gather.9.cloned.1.call-start
  6.5 0.7 all-gather.9.cloned.1.call-update
  7.3 0.0 all-gather.7.cloned.1.call-start
  7.3 1.2 fusion.1
  8.5 2.0 fusion.3
  10.6 0.0 all-gather.7.cloned.1.call-update
  10.6 0.0 all-gather.11.cloned.1.call-start
  10.6 0.7 all-gather.11.cloned.1.call-update
  11.3 0.0 reduce-scatter.3.cloned.1.call-start
  11.5 0.1 broadcast_bitcast_fusion
  11.5 0.1 broadcast_bitcast_fusion.1
  11.6 0.1 broadcast_bitcast_fusion.2
  11.7 0.1 broadcast_bitcast_fusion.3
  11.7 27.9 %all-gather.9.cloned.1.call-done = bf16[2048,256]{1,0:T(8,128)(2,1)} async-done(((bf16[512,256]{1,0:T(8,128)(2,1)}), bf16[2048,256]{1,0:T(8,128)(2,1)}) %all-gather.9.cloned.1.call-update) | async-done | bytes 1048592 | tf_op jit(solution)/shard_map/all_gather | solution.py:56
  39.6 23.5 %all-gather.7.cloned.1.call-done = bf16[512,2048]{1,0:T(8,128)(2,1)} async-done(((bf16[128,2048]{1,0:T(8,128)(2,1)}), bf16[512,2048]{1,0:T(8,128)(2,1)}) %all-gather.7.cloned.1.call-update) | async-done | bytes 2097168 | tf_op jit(solution)/shard_map/all_gather | solution.py:58
  63.2 2.6 fusion
  65.7 0.1 fusion.4
  65.8 0.1 fusion.5
  65.9 0.1 fusion.6
  65.9 0.0 copy-done
  65.9 0.0 copy-start.4
  66.0 0.7 fusion.13
  66.6 0.0 copy-done.4
  66.6 0.1 fusion.11
  66.8 26.0 %all-gather.11.cloned.1.call-done = bf16[256,2048]{1,0:T(8,128)(2,1)} async-done(((bf16[256,512]{1,0:T(8,128)(2,1)}), bf16[256,2048]{1,0:T(8,128)(2,1)}) %all-gather.11.cloned.1.call-update) | async-done | bytes 1048592 | tf_op jit(solution)/shard_map/all_gather | solution.py:63
  92.8 3.3 convolution_convert_fusion
  96.1 0.0 copy-start.1
  96.1 0.0 copy-start.3
  96.1 0.0 reduce-scatter.3.cloned.1.call-update
  96.1 0.0 all-gather.13.cloned.1.call-start
  96.1 30.7 %reduce-scatter.3.cloned.1.call-done = bf16[128,2048]{1,0:T(8,128)(2,1)} async-done(((bf16[512,2048]{1,0:T(8,128)(2,1)}), bf16[128,2048]{1,0:T(8,128)(2,1)}) %reduce-scatter.3.cloned.1.call-update) | async-done | bytes 524304 | tf_op jit(solution)/shard_map/reduce_scatter | solution.py:65
  126.8 0.0 copy-done.1
  126.8 1.3 multiply_reduce_fusion
  128.1 0.0 copy-done.3
  128.1 2.0 multiply_convert_fusion.1
  130.2 0.0 all-gather.13.cloned.1.call-update
  130.2 0.0 all-gather.15.cloned.1.call-start
  130.2 0.5 all-gather.15.cloned.1.call-update
  130.8 0.0 all-gather.17.cloned.1.call-start
  130.8 0.7 all-gather.17.cloned.1.call-update
  131.5 0.0 reduce-scatter.5.cloned.1.call-start
  131.6 21.3 %all-gather.13.cloned.1.call-done = bf16[512,2048]{1,0:T(8,128)(2,1)} async-done(((bf16[128,2048]{1,0:T(8,128)(2,1)}), bf16[512,2048]{1,0:T(8,128)(2,1)}) %all-gather.13.cloned.1.call-update) | async-done | bytes 2097168 | tf_op jit(solution)/shard_map/all_gather | solution.py:75
  152.9 151.1 %all-gather.15.cloned.1.call-done = bf16[2048,2048]{1,0:T(8,128)(2,1)} async-done(((bf16[512,2048]{1,0:T(8,128)(2,1)}), bf16[2048,2048]{1,0:T(8,128)(2,1)}) %all-gather.15.cloned.1.call-update) | async-done | bytes 8388624 | tf_op jit(solution)/shard_map/all_gather | solution.py:73
  304.0 149.4 %all-gather.17.cloned.1.call-done = bf16[2048,2048]{1,0:T(8,128)(2,1)} async-done(((bf16[2048,512]{1,0:T(8,128)(2,1)}), bf16[2048,2048]{1,0:T(8,128)(2,1)}) %all-gather.17.cloned.1.call-update) | async-done | bytes 8388624 | tf_op jit(solution)/shard_map/all_gather | solution.py:80
  453.4 16.5 %convolution_convert_fusion.1 = bf16[512,2048]{1,0:T(8,128)(2,1)} fusion(bf16[2048,2048]{1,0:T(8,128)(2,1)} %all-gather.17.cloned.1.call-done, bf16[512,2048]{1,0:T(8,128)(2,1)} %all-gather.13.cloned.1.call-done, bf16[2048,2048]{1,0:T(8,128)(2,1)} %all-gather.15.cloned.1.call-done), kind=kOutput, calls=%fused_computation.2 | convolution fusion | flops 8594128896 | bytes 20971520 | tf_op jit(solution)/shard_map/dot_general | solution.py:83
  469.9 0.0 copy-start.2
  469.9 0.0 reduce-scatter.5.cloned.1.call-update
  469.9 29.5 %reduce-scatter.5.cloned.1.call-done = bf16[128,2048]{1,0:T(8,128)(2,1)} async-done(((bf16[512,2048]{1,0:T(8,128)(2,1)}), bf16[128,2048]{1,0:T(8,128)(2,1)}) %reduce-scatter.5.cloned.1.call-update) | async-done | bytes 524304 | tf_op jit(solution)/shard_map/reduce_scatter | solution.py:82
  499.4 0.0 copy-done.2
  499.4 2.1 add_convert_fusion
  (6 shorter events, 0.1 us)
Async XLA Ops:
  6.5 59.4 %copy-start = (bf16[2,128,128]{2,1,0:T(8,128)(2,1)S(1)}, bf16[2,128,128]{2,1,0:T(8,128)(2,1)}, u32[]{:S(2)}) copy-start(bf16[2,128,128]{2,1,0:T(8,128)(2,1)} %param.12) | copy-start | bytes 196612
  6.5 33.1 %all-gather.9.cloned.1.call-start = ((), (), s32[]{:S(2)}) async-start(), calls=%async_computation.3 | async-start | bytes 1310720 | tf_op jit(solution)/shard_map/all_gather | solution.py:56
  7.3 55.9 %all-gather.7.cloned.1.call-start = ((), (), s32[]{:S(2)}) async-start(), calls=%async_computation.2 | async-start | bytes 2621440 | tf_op jit(solution)/shard_map/all_gather | solution.py:58
  10.6 82.2 %all-gather.11.cloned.1.call-start = ((), (), s32[]{:S(2)}) async-start(), calls=%async_computation.4 | async-start | bytes 1310720 | tf_op jit(solution)/shard_map/all_gather | solution.py:63
  11.3 115.5 %reduce-scatter.3.cloned.1.call-start = ((), (), s32[]{:S(2)}) async-start(), calls=%async_computation.5 | async-start | bytes 2621440 | tf_op jit(solution)/shard_map/reduce_scatter | solution.py:65
  65.9 0.7 copy-start.4
  96.1 30.8 %copy-start.1 = (bf16[128,2048]{1,0:T(8,128)(2,1)S(1)}, bf16[128,2048]{1,0:T(8,128)(2,1)}, u32[]{:S(2)}) copy-start(bf16[128,2048]{1,0:T(8,128)(2,1)} %param.9) | copy-start | bytes 1572868
  96.1 32.1 %copy-start.3 = (f32[2048]{0:T(1024)S(1)}, f32[2048]{0:T(1024)}, u32[]{:S(2)}) copy-start(f32[2048]{0:T(1024)} %param.15) | copy-start | bytes 24580
  96.1 56.8 %all-gather.13.cloned.1.call-start = ((), (), s32[]{:S(2)}) async-start(), calls=%async_computation.6 | async-start | bytes 2621440 | tf_op jit(solution)/shard_map/all_gather | solution.py:75
  130.2 173.8 %all-gather.15.cloned.1.call-start = ((), (), s32[]{:S(2)}) async-start(), calls=%async_computation.7 | async-start | bytes 10485760 | tf_op jit(solution)/shard_map/all_gather | solution.py:73
  130.8 322.6 %all-gather.17.cloned.1.call-start = ((), (), s32[]{:S(2)}) async-start(), calls=%async_computation.8 | async-start | bytes 10485760 | tf_op jit(solution)/shard_map/all_gather | solution.py:80
  131.5 367.9 %reduce-scatter.5.cloned.1.call-start = ((), (), s32[]{:S(2)}) async-start(), calls=%async_computation.9 | async-start | bytes 2621440 | tf_op jit(solution)/shard_map/reduce_scatter | solution.py:82
  469.9 29.5 %copy-start.2 = (bf16[128,2048]{1,0:T(8,128)(2,1)S(1)}, bf16[128,2048]{1,0:T(8,128)(2,1)}, u32[]{:S(2)}) copy-start(bf16[128,2048]{1,0:T(8,128)(2,1)} %reduce-scatter.3.cloned.1.call-done) | copy-start | bytes 1572868
Sparse Core Ops, SparseCore 0:
  8.9 30.6 all-gather.8
  41.2 21.9 all-gather.6
  64.7 27.9 all-gather.10
  96.2 30.5 reduce-scatter.2
  130.3 22.5 all-gather.12
  154.3 149.5 all-gather.14
  305.5 147.7 all-gather.16
  470.0 29.3 reduce-scatter.4
where the time goes:
time: 509 us; the launch traced here: 508 us
  waiting for transfers between devices  462 us (91%)
  matrix products  23 us (5%)
  between operations  13.6 us (3%)
  other arithmetic  9 us (2%)
    all_gather x1, waiting for transfers between devices, local(): up_local = lax.all_gather(up_weight, 'fs', axis=0, tiled=True)  151 us
    all_gather x1, waiting for transfers between devices, local(): down_local = lax.all_gather(down_weight, 'fs', axis=1, tiled=True)  149 us
    reduce_scatter x1, waiting for transfers between devices, local(): lax.psum_scatter(jnp.dot(block_rows, out_local, preferred_element_type=jn...  30.7 us
    reduce_scatter x1, waiting for transfers between devices, local(): lax.psum_scatter(jnp.dot(block_rows, down_local, preferred_element_type=j...  29.5 us
    all_gather x1, waiting for transfers between devices, local(): in_local = lax.all_gather(in_weight, 'fs', axis=0, tiled=True)  27.9 us
    all_gather x1, waiting for transfers between devices, local(): out_local = lax.all_gather(out_weight, 'fs', axis=1, tiled=True)  26 us
    all_gather x1, waiting for transfers between devices, local(): lax.all_gather(normed, 'tp', axis=0, tiled=True)  23.5 us
    all_gather x1, waiting for transfers between devices, local(): lax.all_gather(normed_two, 'tp', axis=0, tiled=True)  21.3 us
  transfers between devices with their start and end apart: 8, of which 8 were waited for; matrix products, arithmetic and copies ran while one was open for 1% of the time, Pallas kernels for 0%

commit v1 on v0

--- a/solution.py
+++ b/solution.py
@@ -77,7 +77,14 @@
         preferred_element_type=jnp.float32,
     )
     hidden = jnp.square(jax.nn.relu(upper)).astype(jnp.bfloat16)
-    down_local = lax.all_gather(down_weight, "fs", axis=1, tiled=True)
+    size = lax.axis_size("fs")
+    right = [(i, (i + 1) % size) for i in range(size)]
+    parts = [down_weight]
+    for hop in range(1, size):
+        parts = [lax.ppermute(parts[0], "fs", right), *parts]
+    whole = jnp.concatenate(parts, axis=1)
+    turn = (lax.axis_index("fs") + 1) * parts[-1].shape[1]
+    down_local = jnp.roll(whole, turn, axis=1)
     block_rows = hidden
     channel_sum = lax.psum_scatter(
         jnp.dot(block_rows, down_local, preferred_element_type=jnp.float32).astype(jnp.bfloat16),

time: 509 us -> 479 us (0.941)
  waiting for transfers between devices: 462 us -> 346 us
  starting transfers between devices: 0.28 us -> 66.8 us
  local copies, waits for them, and re-layouts: 0.31 us -> 20.2 us
    ppermute x0 -> x3, waiting for transfers between devices: none -> 206 us  [local(): parts = [lax.ppermute(parts[0], 'fs', right), *parts]]
    all_gather x1, waiting for transfers between devices: 151 us -> 0.01 us  [local(): up_local = lax.all_gather(up_weight, 'fs', axis=0, tiled=True)]
    all_gather x1 -> x0, waiting for transfers between devices: 149 us -> none  [local(): down_local = lax.all_gather(down_weight, 'fs', axis=1, tiled=True)]
    ppermute x0 -> x3, starting transfers between devices: none -> 66.6 us  [local(): parts = [lax.ppermute(parts[0], 'fs', right), *parts]]
    all_gather x1, waiting for transfers between devices: 21.3 us -> 0.01 us  [local(): lax.all_gather(normed_two, 'tp', axis=0, tiled=True)]
    unnamed x10 -> x23, local copies, waits for them, and re-layouts: 0.02 us -> 18.4 us
  transfers between devices with their start and end apart: 8 -> 10, of which waited for: 8 -> 8; matrix products, arithmetic and copies ran while one was open for 1% -> 5% of each run, Pallas kernels for 0% -> 0%
where the time goes in v1:
time: 479 us; the launch traced here: 478 us
  waiting for transfers between devices  346 us (72%)
  starting transfers between devices  66.8 us (14%)
  matrix products  23.1 us (5%)
  local copies, waits for them, and re-layouts  20.2 us (4%)
  between operations  13.6 us (3%)
  other arithmetic  8.99 us (2%)
    ppermute x3, waiting for transfers between devices, local(): parts = [lax.ppermute(parts[0], 'fs', right), *parts]  206 us
    ppermute x3, starting transfers between devices, local(): parts = [lax.ppermute(parts[0], 'fs', right), *parts]  66.6 us
    reduce_scatter x1, waiting for transfers between devices, local(): lax.psum_scatter(jnp.dot(block_rows, out_local, preferred_element_type=jn...  30.7 us
    reduce_scatter x1, waiting for transfers between devices, local(): lax.psum_scatter(jnp.dot(block_rows, down_local, preferred_element_type=j...  29.2 us
    all_gather x1, waiting for transfers between devices, local(): in_local = lax.all_gather(in_weight, 'fs', axis=0, tiled=True)  27.9 us
    all_gather x1, waiting for transfers between devices, local(): out_local = lax.all_gather(out_weight, 'fs', axis=1, tiled=True)  26 us
    all_gather x1, waiting for transfers between devices, local(): lax.all_gather(normed, 'tp', axis=0, tiled=True)  23.5 us
    unnamed x23, local copies, waits for them, and re-layouts  18.4 us
  transfers between devices with their start and end apart: 10, of which 8 were waited for; matrix products, arithmetic and copies ran while one was open for 5% of the time, Pallas kernels for 0%

profile of v1, /device:TPU:0, one launch (start us, length us, event | category | flops | bytes accessed | tf_op | source)
XLA Modules:
  0.0 478.3 jit_solution(14175025263981945486)
XLA Ops:
  6.5 0.0 copy-start
  6.5 0.0 all-gather.8.cloned.1.call-start
  6.5 0.7 all-gather.8.cloned.1.call-update
  7.3 0.0 all-gather.6.cloned.1.call-start
  7.3 1.2 fusion.6
  8.5 2.0 fusion.8
  10.6 0.0 all-gather.6.cloned.1.call-update
  10.6 0.0 all-gather.10.cloned.1.call-start
  10.6 0.7 all-gather.10.cloned.1.call-update
  11.3 0.0 reduce-scatter.3.cloned.1.call-start
  11.5 0.1 broadcast_bitcast_fusion
  11.5 0.1 broadcast_bitcast_fusion.1
  11.6 0.1 broadcast_bitcast_fusion.2
  11.7 0.1 broadcast_bitcast_fusion.3
  11.7 27.9 %all-gather.8.cloned.1.call-done = bf16[2048,256]{1,0:T(8,128)(2,1)} async-done(((bf16[512,256]{1,0:T(8,128)(2,1)}), bf16[2048,256]{1,0:T(8,128)(2,1)}) %all-gather.8.cloned.1.call-update) | async-done | bytes 1048592 | tf_op jit(solution)/shard_map/all_gather | solution.py:56
  39.6 23.5 %all-gather.6.cloned.1.call-done = bf16[512,2048]{1,0:T(8,128)(2,1)} async-done(((bf16[128,2048]{1,0:T(8,128)(2,1)}), bf16[512,2048]{1,0:T(8,128)(2,1)}) %all-gather.6.cloned.1.call-update) | async-done | bytes 2097168 | tf_op jit(solution)/shard_map/all_gather | solution.py:58
  63.2 2.6 fusion.5
  65.7 0.1 fusion.9
  65.8 0.1 fusion.10
  65.9 0.1 fusion.11
  65.9 0.0 copy-done
  65.9 0.0 copy-start.7
  66.0 0.7 fusion.18
  66.6 0.0 copy-done.7
  66.6 0.0 copy-start.1
  66.7 0.0 copy-start.6
  66.7 0.1 fusion.16
  66.8 26.0 %all-gather.10.cloned.1.call-done = bf16[256,2048]{1,0:T(8,128)(2,1)} async-done(((bf16[256,512]{1,0:T(8,128)(2,1)}), bf16[256,2048]{1,0:T(8,128)(2,1)}) %all-gather.10.cloned.1.call-update) | async-done | bytes 1048592 | tf_op jit(solution)/shard_map/all_gather | solution.py:63
  92.8 3.3 convolution_convert_fusion
  96.1 0.0 copy-start.2
  96.1 0.0 reduce-scatter.3.cloned.1.call-update
  96.1 0.0 all-gather.12.cloned.1.call-start
  96.1 30.7 %reduce-scatter.3.cloned.1.call-done = bf16[128,2048]{1,0:T(8,128)(2,1)} async-done(((bf16[512,2048]{1,0:T(8,128)(2,1)}), bf16[128,2048]{1,0:T(8,128)(2,1)}) %reduce-scatter.3.cloned.1.call-update) | async-done | bytes 524304 | tf_op jit(solution)/shard_map/reduce_scatter | solution.py:65
  126.8 0.0 copy-done.1
  126.8 1.3 multiply_reduce_fusion
  128.1 0.0 copy-done.6
  128.1 2.0 multiply_convert_fusion.1
  130.2 0.0 all-gather.12.cloned.1.call-update
  130.2 0.0 all-gather.14.cloned.1.call-start
  130.2 0.5 all-gather.14.cloned.1.call-update
  130.8 0.0 reduce-scatter.5.cloned.1.call-start
  130.8 0.0 copy-done.2
  130.8 1.5 collective-permute-start
  132.3 60.4 %collective-permute-done = bf16[2048,512]{1,0:T(8,128)(2,1)S(1)} collective-permute-done((bf16[2048,512]{1,0:T(8,128)(2,1)S(1)}, bf16[2048,512]{1,0:T(8,128)(2,1)S(1)}, u32[]{:S(2)}, u32[]{:S(2)}) %collective-permute-start) | collective-permute-done | bytes 2097184 | tf_op jit(solution)/shard_map/ppermute | solution.py:84
  192.8 0.0 copy-start.3
  192.8 1.3 copy-done.3
  194.1 15.6 %collective-permute-start.1 = (bf16[2048,512]{1,0:T(8,128)(2,1)S(1)}, bf16[2048,512]{1,0:T(8,128)(2,1)}, u32[]{:S(2)}, u32[]{:S(2)}) collective-permute-start(bf16[2048,512]{1,0:T(8,128)(2,1)S(1)} %collective-permute-done), channel_id=1, source_target_pairs={{0,4},{4,8},{8,12},{12,0},{1,5},{5,9},{9,13},{13,1},{2,6},{6,10},{... | collective-permute-start | bytes 6291464 | tf_op jit(solution)/shard_map/ppermute | solution.py:84
  209.7 89.2 %collective-permute-done.1 = bf16[2048,512]{1,0:T(8,128)(2,1)} collective-permute-done((bf16[2048,512]{1,0:T(8,128)(2,1)S(1)}, bf16[2048,512]{1,0:T(8,128)(2,1)}, u32[]{:S(2)}, u32[]{:S(2)}) %collective-permute-start.1) | collective-permute-done | bytes 2097184 | tf_op jit(solution)/shard_map/ppermute | solution.py:84
  298.8 49.4 %collective-permute-start.2 = (bf16[2048,512]{1,0:T(8,128)(2,1)}, bf16[2048,512]{1,0:T(8,128)(2,1)}, u32[]{:S(2)}, u32[]{:S(2)}) collective-permute-start(bf16[2048,512]{1,0:T(8,128)(2,1)} %collective-permute-done.1), channel_id=1, source_target_pairs={{0,4},{4,8},{8,12},{12,0},{1,5},{5,9},{9,13},{13,1},{2,6},{6,10},{... | collective-permute-start | bytes 6291464 | tf_op jit(solution)/shard_map/ppermute | solution.py:84
  348.3 56.7 %collective-permute-done.2 = bf16[2048,512]{1,0:T(8,128)(2,1)} collective-permute-done((bf16[2048,512]{1,0:T(8,128)(2,1)}, bf16[2048,512]{1,0:T(8,128)(2,1)}, u32[]{:S(2)}, u32[]{:S(2)}) %collective-permute-start.2) | collective-permute-done | bytes 2097184 | tf_op jit(solution)/shard_map/ppermute | solution.py:84
  405.0 3.1 constant_dynamic-update-slice_fusion.7
  408.1 3.1 constant_dynamic-update-slice_fusion.6
  411.2 0.0 copy-done.4
  411.2 1.5 constant_dynamic-update-slice_fusion.5
  412.7 1.5 constant_dynamic-update-slice_fusion.4
  414.3 3.1 constant_dynamic-update-slice_fusion.3
  417.4 3.1 constant_dynamic-update-slice_fusion.2
  420.5 1.5 constant_dynamic-update-slice_fusion.1
  422.0 1.5 constant_dynamic-update-slice_fusion
  423.5 16.6 %fusion.2 = bf16[512,2048]{1,0:T(8,128)(2,1)} fusion(bf16[2048,4096]{1,0:T(8,128)(2,1)} %constant_dynamic-update-slice_fusion, s32[]{:T(128)S(6)} %select_n.38, bf16[512,2048]{1,0:T(8,128)(2,1)} %all-gather.12.cloned.1.call-done, bf16[2048,2048]{1,0:T(8,128)(2,1)} %all-gather.14.cloned.1.call-done), kind=kOutput, calls=%fused_computation.4 | convolution fusion | flops 8594128896 | bytes 20971524 | tf_op jit(solution)/shard_map/dot_general | solution.py:90
  440.1 0.0 reduce-scatter.5.cloned.1.call-update
  440.2 29.2 %reduce-scatter.5.cloned.1.call-done = bf16[128,2048]{1,0:T(8,128)(2,1)} async-done(((bf16[512,2048]{1,0:T(8,128)(2,1)}), bf16[128,2048]{1,0:T(8,128)(2,1)}) %reduce-scatter.5.cloned.1.call-update) | async-done | bytes 524304 | tf_op jit(solution)/shard_map/reduce_scatter | solution.py:89
  469.4 0.0 copy-done.5
  469.4 2.1 add_convert_fusion
  (10 shorter events, 0.1 us)
Async XLA Ops:
  6.5 59.4 %copy-start = (bf16[2,128,128]{2,1,0:T(8,128)(2,1)S(1)}, bf16[2,128,128]{2,1,0:T(8,128)(2,1)}, u32[]{:S(2)}) copy-start(bf16[2,128,128]{2,1,0:T(8,128)(2,1)} %param.12) | copy-start | bytes 196612
  6.5 33.1 %all-gather.8.cloned.1.call-start = ((), (), s32[]{:S(2)}) async-start(), calls=%async_computation.3 | async-start | bytes 1310720 | tf_op jit(solution)/shard_map/all_gather | solution.py:56
  7.3 55.9 %all-gather.6.cloned.1.call-start = ((), (), s32[]{:S(2)}) async-start(), calls=%async_computation.2 | async-start | bytes 2621440 | tf_op jit(solution)/shard_map/all_gather | solution.py:58
  10.6 82.2 %all-gather.10.cloned.1.call-start = ((), (), s32[]{:S(2)}) async-start(), calls=%async_computation.4 | async-start | bytes 1310720 | tf_op jit(solution)/shard_map/all_gather | solution.py:63
  11.3 115.5 %reduce-scatter.3.cloned.1.call-start = ((), (), s32[]{:S(2)}) async-start(), calls=%async_computation.5 | async-start | bytes 2621440 | tf_op jit(solution)/shard_map/reduce_scatter | solution.py:65
  65.9 0.7 copy-start.7
  66.6 60.2 %copy-start.1 = (bf16[128,2048]{1,0:T(8,128)(2,1)S(1)}, bf16[128,2048]{1,0:T(8,128)(2,1)}, u32[]{:S(2)}) copy-start(bf16[128,2048]{1,0:T(8,128)(2,1)} %param.9) | copy-start | bytes 1572868
  66.7 61.5 %copy-start.6 = (f32[2048]{0:T(1024)S(1)}, f32[2048]{0:T(1024)}, u32[]{:S(2)}) copy-start(f32[2048]{0:T(1024)} %param.15) | copy-start | bytes 24580
  96.1 34.8 %copy-start.2 = (bf16[2048,512]{1,0:T(8,128)(2,1)S(1)}, bf16[2048,512]{1,0:T(8,128)(2,1)}, u32[]{:S(2)}) copy-start(bf16[2048,512]{1,0:T(8,128)(2,1)} %param.17) | copy-start | bytes 6291460
  96.1 327.5 %all-gather.12.cloned.1.call-start = ((), (), s32[]{:S(2)}) async-start(), calls=%async_computation.6 | async-start | bytes 2621440 | tf_op jit(solution)/shard_map/all_gather | solution.py:75
  130.2 293.4 %all-gather.14.cloned.1.call-start = ((), (), s32[]{:S(2)}) async-start(), calls=%async_computation.7 | async-start | bytes 10485760 | tf_op jit(solution)/shard_map/all_gather | solution.py:73
  130.8 338.6 %reduce-scatter.5.cloned.1.call-start = ((), (), s32[]{:S(2)}) async-start(), calls=%async_computation.8 | async-start | bytes 2621440 | tf_op jit(solution)/shard_map/reduce_scatter | solution.py:89
  130.8 61.9 %collective-permute-start = (bf16[2048,512]{1,0:T(8,128)(2,1)S(1)}, bf16[2048,512]{1,0:T(8,128)(2,1)S(1)}, u32[]{:S(2)}, u32[]{:S(2)}) collective-permute-start(bf16[2048,512]{1,0:T(8,128)(2,1)S(1)} %copy-done.2), channel_id=1, source_target_pairs={{0,4},{4,8},{8,12},{12,0},{1,5},{5,9},{9,13},{13,1},{2,6},{6,10},{... | collective-permute-start | bytes 6291464 | tf_op jit(solution)/shard_map/ppermute | solution.py:84
  192.8 1.3 copy-start.3
  194.1 104.8 %collective-permute-start.1 = (bf16[2048,512]{1,0:T(8,128)(2,1)S(1)}, bf16[2048,512]{1,0:T(8,128)(2,1)}, u32[]{:S(2)}, u32[]{:S(2)}) collective-permute-start(bf16[2048,512]{1,0:T(8,128)(2,1)S(1)} %collective-permute-done), channel_id=1, source_target_pairs={{0,4},{4,8},{8,12},{12,0},{1,5},{5,9},{9,13},{13,1},{2,6},{6,10},{... | collective-permute-start | bytes 6291464 | tf_op jit(solution)/shard_map/ppermute | solution.py:84
  298.8 106.2 %collective-permute-start.2 = (bf16[2048,512]{1,0:T(8,128)(2,1)}, bf16[2048,512]{1,0:T(8,128)(2,1)}, u32[]{:S(2)}, u32[]{:S(2)}) collective-permute-start(bf16[2048,512]{1,0:T(8,128)(2,1)} %collective-permute-done.1), channel_id=1, source_target_pairs={{0,4},{4,8},{8,12},{12,0},{1,5},{5,9},{9,13},{13,1},{2,6},{6,10},{... | collective-permute-start | bytes 6291464 | tf_op jit(solution)/shard_map/ppermute | solution.py:84
  348.3 62.9 %copy-start.4 = (bf16[2048,512]{1,0:T(8,128)(2,1)S(1)}, bf16[2048,512]{1,0:T(8,128)(2,1)}, u32[]{:S(2)}) copy-start(bf16[2048,512]{1,0:T(8,128)(2,1)} %copy-done.3) | copy-start | bytes 6291460
  423.5 45.9 %copy-start.5 = (bf16[128,2048]{1,0:T(8,128)(2,1)S(1)}, bf16[128,2048]{1,0:T(8,128)(2,1)}, u32[]{:S(2)}) copy-start(bf16[128,2048]{1,0:T(8,128)(2,1)} %reduce-scatter.3.cloned.1.call-done) | copy-start | bytes 1572868
Sparse Core Ops, SparseCore 0:
  8.9 30.6 all-gather.7
  41.2 21.9 all-gather.5
  64.7 27.9 all-gather.9
  96.2 30.5 reduce-scatter.2
  130.3 22.5 all-gather.11
  154.3 220.4 all-gather.13
  440.3 29.0 reduce-scatter.4
